TPU v7x, 32 devices: a whole 2x2x4 slice. The times are simulated.
32 devices in a mesh: kv: 16 (over z, y, core), tp: 2 (over x).
Axes of the slice: x: 2, y: 2, z: 4, core: 2. Of those that a mesh axis runs over, the one named last changes fastest.
Arguments:
- queries: bfloat16 [4096, 1536], P('kv', 'tp'), may hold values from -6 to 6
- keys: bfloat16 [4096, 256], P('kv', 'tp'), may hold values from -6 to 6
- values: bfloat16 [4096, 256], P('kv', 'tp'), may hold values from -6 to 6
- log_sums: float32 [12, 4096], P('tp', 'kv'), may hold values from 6 to 7.5
- out_grad: bfloat16 [4096, 1536], P('kv', 'tp'), may hold values from -6 to 6
- chosen: int32 [64, 2, 8], P('kv', 'tp'), may hold values from 0 to 63, as said below
- inputs: bfloat16 [4096, 3072], P('kv', 'tp'), may hold values from -6 to 6
Outputs:
- query_grad: bfloat16 [4096, 1536], P('kv', 'tp')
- key_grad: bfloat16 [4096, 256], P('kv', 'tp')
- value_grad: bfloat16 [4096, 256], P('kv', 'tp')
- weight_grad: float32 [3072, 256], P('kv', 'tp')
Inputs may be any that keep to these rules, and one draw needn't show every extreme that they name: `chosen`: for query block g and key head h, every slot holds g (an empty slot) or a key block c with g - 16 <= c < g; the blocks of the live slots of one list are distinct; each list has between 4 and 8 live slots, except that query block g has at most g of them (block 0 has none).
All inputs are finite; a program needn't handle non-finite values.
Results may differ from a plain program's by a relative error of at most 0.0049.
Values may be sent and summed in bfloat16 or wider, within the bound.
A program may use at most 64 MiB of HBM per device.

v0:
```python
import functools

import jax
import jax.numpy as jnp
from jax import lax
from jax.experimental import pallas as pl
from jax.experimental.pallas import tpu as pltpu
from jax.sharding import PartitionSpec as P

REACH = 4
MASKED = -1e30
LOG2E = 1.4426950408889634
MESH = pl.DeviceIdType.MESH
NT = (((1,), (1,)), ((), ()))


def kernel(
    nk,
    nt,
    chosen_ref,
    lse_ref,
    k_ref,
    v_ref,
    q_hbm,
    do_hbm,
    x_hbm,
    qg_ref,
    kg_ref,
    vg_ref,
    wg_ref,
    q_s,
    do_s,
    x_s,
    q6,
    do6,
    kw,
    vw,
    kt,
    bias_ref,
    own_bias,
    p_s,
    pb_s,
    ds_s,
    dvo,
    dvi,
    dko,
    dki,
    dv_own,
    x_t,
    x_in,
    vpair,
    po,
    ri,
    ld_sem,
    k_send,
    k_recv,
    v_send,
    v_recv,
    dv_send,
    dv_recv,
    dk_send,
    dk_recv,
    x_send,
    x_recv,
    x_loc,
    vp_send,
    vp_recv,
    rs_send,
    rs_recv,
):
    me = lax.axis_index("kv")
    tp = lax.axis_index("tp")
    core = lax.rem(me, 2)
    chip = me // 2
    sib = me + 1 - 2 * core
    chips = nk // 2
    tok, hd = k_ref.shape
    heads = lse_ref.shape[0]
    nblk = chosen_ref.shape[0]
    blk = tok // nblk
    scale = hd**-0.5
    per_tp, _, rw, _ = x_t.shape

    loads = [
        pltpu.make_async_copy(src, dst, ld_sem.at[i])
        for i, (src, dst) in enumerate(((x_hbm, x_s), (q_hbm, q_s), (do_hbm, do_s)))
    ]
    for load in loads:
        load.start()

    barrier = pltpu.get_barrier_semaphore()

    @pl.loop(1, nk)
    def _(j):
        pl.semaphore_signal(
            barrier, inc=1, device_id=(lax.rem(me + j, nk), tp), device_id_type=MESH
        )

    for dt in range(1, nt):
        for kv in (me, sib):
            pl.semaphore_signal(
                barrier, inc=1, device_id=(kv, lax.rem(tp + dt, nt)), device_id_type=MESH
            )
    pl.semaphore_wait(barrier, nk - 1 + 2 * (nt - 1))

    def remote(src, dst, send, recv, kv, t=None):
        return pltpu.make_async_remote_copy(
            src_ref=src,
            dst_ref=dst,
            send_sem=send,
            recv_sem=recv,
            device_id=(kv, tp if t is None else t),
            device_id_type=MESH,
        )

    def k_copy(o):
        return remote(k_ref, kw.at[o], k_send.at[o], k_recv.at[o], me + o)

    def v_copy(o):
        return remote(v_ref, vw.at[o], v_send.at[o], v_recv.at[o], me + o)

    def dv_copy(o):
        return remote(dvo.at[o], dvi.at[o], dv_send.at[o], dv_recv.at[o], me - o)

    def dk_copy(o):
        return remote(dko.at[o], dki.at[o], dk_send.at[o], dk_recv.at[o], me - o)

    for copy in (k_copy, v_copy):
        for o in range(1, REACH + 1):

            @pl.when(me + o < nk)
            def _():
                copy(o).start()

    loads[0].wait()
    x_t[...] = x_s[...].T.reshape(x_t.shape)
    half = per_tp // 2
    x_copies = []
    for h in range(2):
        rows = pl.ds(h * half, half)
        for dt in range(1, nt):
            other = lax.rem(tp + dt, nt)
            for s, kv, par in ((0, me, core), (1, sib, 1 - core)):
                x_copies.append(
                    remote(
                        x_t.at[rows, par],
                        x_in.at[tp, core, rows],
                        x_send.at[h, dt, s],
                        x_recv.at[h, tp, core],
                        kv,
                        other,
                    )
                )
        x_copies.append(
            remote(
                x_t.at[rows, 1 - core],
                x_in.at[tp, core, rows],
                x_send.at[h, 0, 1],
                x_recv.at[h, tp, core],
                sib,
            )
        )
    for copy in x_copies:
        copy.start()
    x_local = pltpu.make_async_copy(x_t.at[:, core], x_in.at[tp, core], x_loc)
    x_local.start()

    zero = jnp.zeros((tok, hd), jnp.bfloat16)
    for o in range(1, REACH + 1):

        @pl.when(me < o)
        def _():
            kw[o] = zero
            vw[o] = zero

        @pl.when(me + o >= nk)
        def _():
            dvi[o] = zero
            dki[o] = zero

    kw[0] = k_ref[...]
    vw[0] = v_ref[...]
    loads[1].wait()
    loads[2].wait()
    for a in range(heads):
        q6[a] = q_s[:, a * hd : (a + 1) * hd]
        do6[a] = do_s[:, a * hd : (a + 1) * hd]
    row = lax.broadcasted_iota(jnp.int32, (nblk, tok), 0)
    col = lax.broadcasted_iota(jnp.int32, (nblk, tok), 1)
    marked = [jnp.full((nblk, tok), MASKED, jnp.float32) for _ in range(REACH + 1)]
    for b in range(nblk):
        in_block = (col >= b * blk) & (col < (b + 1) * blk)
        marked[0] = jnp.where(in_block & (row == b), 0.0, marked[0])
        for slot in range(chosen_ref.shape[2]):
            block = chosen_ref[b, 0, slot]
            block = jnp.where(block < me * nblk + b, block, -1)
            for o in range(REACH + 1):
                hit = in_block & (row + (me - o) * nblk == block)
                marked[o] = jnp.where(hit & (block >= 0), 0.0, marked[o])
    for o in range(REACH + 1):
        bias_ref[o] = marked[o]
    key_row = lax.broadcasted_iota(jnp.int32, (blk, tok), 0)
    pos = lax.broadcasted_iota(jnp.int32, (blk, tok), 1)
    for j in range(nblk):
        own_bias[j * blk : (j + 1) * blk, :] = jnp.where(
            key_row + j * blk > pos, MASKED, bias_ref[0, j : j + 1, :]
        )

    def first(o, own):
        keys = kw[o]
        for a in range(heads):
            s = lax.dot_general(keys, q6[a], NT, preferred_element_type=jnp.float32)
            s = s * (scale * LOG2E)
            lse = lse_ref[a : a + 1, :] * LOG2E
            if own:
                p = jnp.exp2(s + (own_bias[...] - lse))
            else:
                rows = bias_ref[o] - lse
                p = jnp.exp2(s.reshape(nblk, blk, tok) + rows[:, None, :]).reshape(tok, tok)
            p_s[a, o] = p
            pb_s[:, a * tok : (a + 1) * tok] = p.astype(jnp.bfloat16)
        return jnp.dot(
            pb_s[...], do6[...].reshape(heads * tok, hd), preferred_element_type=jnp.float32
        )

    dv_own[...] = first(0, True)

    @pl.loop(1, REACH + 1)
    def _(o):
        @pl.when(me >= o)
        def _():
            k_copy(o).wait_recv()

        dvo[o] = first(o, False).astype(jnp.bfloat16)

        @pl.when(me >= o)
        def _():
            dv_copy(o).start()

    kt[...] = kw[...].reshape((REACH + 1) * tok, hd).T
    for o in range(1, REACH + 1):

        @pl.when(me >= o)
        def _():
            v_copy(o).wait_recv()

    def score_grad(a):
        gw = lax.dot_general(
            vw[...].reshape((REACH + 1) * tok, hd), do6[a], NT, preferred_element_type=jnp.float32
        )
        p = p_s[a].reshape((REACH + 1) * tok, tok)
        delta = jnp.sum(p * gw, 0, keepdims=True)
        ds_s[:, a * tok : (a + 1) * tok] = (p * (gw - delta)).astype(jnp.bfloat16)

    def query_part(a):
        ds = ds_s[:, a * tok : (a + 1) * tok]
        dq_t = jnp.dot(kt[...], ds, preferred_element_type=jnp.float32) * scale
        qg_ref[:, a * hd : (a + 1) * hd] = dq_t.T.astype(jnp.bfloat16)

    def rs_copy(to):
        return remote(po.at[to], ri.at[chip], rs_send.at[to], rs_recv.at[chip], to * 2 + core)

    def weight_part(dt, h):
        t = lax.rem(tp + dt, nt)
        rows = pl.ds(h * half, half)
        for c in range(2):

            @pl.when((t != tp) | (c != core))
            def _():
                remote(
                    x_t.at[rows, 0],
                    x_in.at[t, c, rows],
                    x_send.at[0, 0, 1],
                    x_recv.at[h, t, c],
                    sib,
                ).wait_recv()

        part = jnp.dot(
            x_in[t, 0, rows].reshape(half * rw, tok), vpair[0], preferred_element_type=jnp.float32
        ) + jnp.dot(
            x_in[t, 1, rows].reshape(half * rw, tok), vpair[1], preferred_element_type=jnp.float32
        )
        start = t * per_tp + h * half
        po[pl.ds(start, half)] = part.astype(jnp.bfloat16).reshape(half, rw, hd)

        @pl.loop(0, half)
        def _(j):
            @pl.when(start + j != chip)
            def _():
                rs_copy(start + j).start()

    split = heads // 2
    for a in range(split):
        score_grad(a)

    value = dv_own[...]
    for o in range(1, REACH + 1):

        @pl.when(me + o < nk)
        def _():
            dv_copy(o).wait_recv()

        value = value + dvi[o].astype(jnp.float32)
    value = value.astype(jnp.bfloat16)
    vg_ref[...] = value
    vpair[pl.ds(core, 1)] = value[None]
    pair = remote(vpair.at[core], vpair.at[core], vp_send, vp_recv, sib)
    pair.start()
    score_grad(split)
    remote(vpair.at[core], vpair.at[1 - core], vp_send, vp_recv, sib).wait_recv()
    x_local.wait()
    for dt in range(1, nt):
        weight_part(dt, 0)
    for h in range(2):
        weight_part(0, h)
    for a in range(split + 1, heads):
        score_grad(a)

    for o in range(REACH, -1, -1):
        dk = (
            jnp.dot(
                ds_s[o * tok : (o + 1) * tok, :],
                q6[...].reshape(heads * tok, hd),
                preferred_element_type=jnp.float32,
            )
            * scale
        )
        if o == 0:
            key = dk
        else:
            dko[o] = dk.astype(jnp.bfloat16)

            @pl.when(me >= o)
            def _():
                dk_copy(o).start()

    for a in range(split):
        query_part(a)
    for dt in range(1, nt):
        weight_part(dt, 1)
    for a in range(split, heads):
        query_part(a)

    ri[pl.ds(chip, 1)] = po[pl.ds(chip, 1)]
    for o in range(1, REACH + 1):

        @pl.when(me + o < nk)
        def _():
            dk_copy(o).wait_recv()

        key = key + dki[o].astype(jnp.float32)
    kg_ref[...] = key.astype(jnp.bfloat16)

    @pl.loop(1, chips)
    def _(j):
        src = lax.rem(chip + j, chips)
        remote(po.at[src], ri.at[src], rs_send.at[src], rs_recv.at[src], src * 2 + core).wait_recv()

    wg_ref[...] = jnp.sum(ri[...].astype(jnp.float32), 0)

    for o in range(1, REACH + 1):

        @pl.when(me + o < nk)
        def _():
            k_copy(o).wait_send()
            v_copy(o).wait_send()

        @pl.when(me >= o)
        def _():
            dv_copy(o).wait_send()
            dk_copy(o).wait_send()

    for copy in x_copies:
        copy.wait_send()
    pair.wait_send()

    @pl.loop(1, chips)
    def _(j):
        rs_copy(lax.rem(chip + j, chips)).wait_send()


def finish(*refs):
    count = len(refs) // 2
    sems = refs[-1]
    copies = [
        pltpu.make_async_copy(refs[i], refs[count + i], sems.at[i]) for i in range(count)
    ]
    for copy in copies:
        copy.start()
    for copy in copies:
        copy.wait()


def shards(nk, nt, queries, keys, values, log_sums, out_grad, chosen, inputs):
    tok, hd = keys.shape
    heads = queries.shape[1] // hd
    nblk = chosen.shape[0]
    feats = inputs.shape[1]
    rw = feats * nt // nk
    per_tp = feats // (2 * rw)
    span = REACH + 1
    bf, f32 = jnp.bfloat16, jnp.float32
    dma = pltpu.SemaphoreType.DMA
    vmem = pl.BlockSpec(memory_space=pltpu.VMEM)
    hbm = pl.BlockSpec(memory_space=pl.ANY)
    parts = pl.pallas_call(
        functools.partial(kernel, nk, nt),
        out_shape=(
            jax.ShapeDtypeStruct((tok, heads * hd), bf),
            jax.ShapeDtypeStruct((tok, hd), bf),
            jax.ShapeDtypeStruct((tok, hd), bf),
            jax.ShapeDtypeStruct((rw, hd), f32),
        ),
        in_specs=[pl.BlockSpec(memory_space=pltpu.SMEM), vmem, vmem, vmem, hbm, hbm, hbm],
        out_specs=(vmem, vmem, vmem, vmem),
        scratch_shapes=[
            pltpu.VMEM((tok, heads * hd), bf),
            pltpu.VMEM((tok, heads * hd), bf),
            pltpu.VMEM((tok, feats), bf),
            pltpu.VMEM((heads, tok, hd), bf),
            pltpu.VMEM((heads, tok, hd), bf),
            pltpu.VMEM((span, tok, hd), bf),
            pltpu.VMEM((span, tok, hd), bf),
            pltpu.VMEM((hd, span * tok), bf),
            pltpu.VMEM((span, nblk, tok), f32),
            pltpu.VMEM((tok, tok), f32),
            pltpu.VMEM((heads, span, tok, tok), f32),
            pltpu.VMEM((tok, heads * tok), bf),
            pltpu.VMEM((span * tok, heads * tok), bf),
            pltpu.VMEM((span, tok, hd), bf),
            pltpu.VMEM((span, tok, hd), bf),
            pltpu.VMEM((span, tok, hd), bf),
            pltpu.VMEM((span, tok, hd), bf),
            pltpu.VMEM((tok, hd), f32),
            pltpu.VMEM((per_tp, 2, rw, tok), bf),
            pltpu.VMEM((nt, 2, per_tp, rw, tok), bf),
            pltpu.VMEM((2, tok, hd), bf),
            pltpu.VMEM((nk // 2, rw, hd), bf),
            pltpu.VMEM((nk // 2, rw, hd), bf),
            dma((3,)),
            dma((span,)),
            dma((span,)),
            dma((span,)),
            dma((span,)),
            dma((span,)),
            dma((span,)),
            dma((span,)),
            dma((span,)),
            dma((2, nt, 2)),
            dma((2, nt, 2)),
            dma,
            dma,
            dma,
            dma((nk // 2,)),
            dma((nk // 2,)),
        ],
        compiler_params=pltpu.CompilerParams(
            collective_id=0, has_side_effects=True, vmem_limit_bytes=60 * 1024 * 1024
        ),
    )(chosen, log_sums, keys, values, queries, out_grad, inputs)
    return pl.pallas_call(
        finish,
        out_shape=tuple(jax.ShapeDtypeStruct(part.shape, part.dtype) for part in parts),
        in_specs=[vmem] * len(parts),
        out_specs=(hbm,) * len(parts),
        scratch_shapes=[dma((len(parts),))],
    )(*parts)


def solution(mesh):
    in_specs = (
        P("kv", "tp"),
        P("kv", "tp"),
        P("kv", "tp"),
        P("tp", "kv"),
        P("kv", "tp"),
        P("kv", "tp", None),
        P("kv", "tp"),
    )
    out_specs = (P("kv", "tp"), P("kv", "tp"), P("kv", "tp"), P("kv", "tp"))
    return jax.shard_map(
        functools.partial(shards, mesh.shape["kv"], mesh.shape["tp"]),
        mesh=mesh,
        in_specs=in_specs,
        out_specs=out_specs,
        check_vma=False,
    )
```

profile of v0, /device:TPU:14, one launch (start us, length us, event | category | flops | bytes accessed | tf_op | source)
XLA Modules:
  0.0 37.0 jit_solution(12240225129630846908)
XLA Ops:
  0.6 34.5 %shard_map.102 = (bf16[256,768]{1,0:T(8,128)(2,1)}, bf16[256,128]{1,0:T(8,128)(2,1)}, bf16[256,128]{1,0:T(8,128)(2,1)}, f32[192,128]{1,0:T(8,128)}) custom-call(s32[4,1,8]{2,1,0:T(1,128)} %chosen_ref.1, f32[6,256]{1,0:T(8,128)} %lse_ref.1, bf16[256,128]{1,0:T(8,128)(2,1)} %k_ref.1, bf16[256,128]{1,0:T(8,128)(2,1)} %v_ref.1, bf16[256,768]{1,0:T(8,128)(2,1)} %q_hbm.1, ...), custom_call_target="tpu_custom_call" | custom-call | tf_op jit(solution)/shard_map/pallas_call | solution.py:406
  35.1 1.9 %shard_map.103 = (bf16[256,768]{1,0:T(8,128)(2,1)}, bf16[256,128]{1,0:T(8,128)(2,1)}, bf16[256,128]{1,0:T(8,128)(2,1)}, f32[192,128]{1,0:T(8,128)}) custom-call(bf16[256,768]{1,0:T(8,128)(2,1)} %get-tuple-element.8.refs_0_, bf16[256,128]{1,0:T(8,128)(2,1)} %get-tuple-element.9.refs_1_, bf16[256,128]{1,0:T(8,128)(2,1)} %get-tuple-element.10.refs_2_, ...), custom_call_target="tpu_custom_call" | custom-call | tf_op jit(solution)/shard_map/pallas_call | solution.py:461
where the time goes:
time: 37.7 us; the launch traced here: 37 us
  Pallas kernels  36.4 us (97%)
  between operations  0.64 us (2%)
    pallas_call x1, Pallas kernels, shards(): pl.pallas_call(functools.partial(kernel, nk, nt), out_shape=(jax.ShapeDty...  34.5 us
    pallas_call x1, Pallas kernels, shards(): pl.pallas_call(finish, out_shape=tuple((jax.ShapeDtypeStruct(part.shape,...  1.93 us

commit v1 on v0

v1 whole, which is shorter than its diff:
```python
import functools

import jax
import jax.numpy as jnp
from jax import lax
from jax.experimental import pallas as pl
from jax.experimental.pallas import tpu as pltpu
from jax.sharding import PartitionSpec as P

REACH = 4
BACK = REACH // 2
SPAN = BACK + 1
MASKED = -1e30
NO_BLOCK = -(1 << 20)
LOG2E = 1.4426950408889634
MESH = pl.DeviceIdType.MESH
NT = (((1,), (1,)), ((), ()))
scope = jax.named_scope


def kernel(
    nk,
    nt,
    chosen_hbm,
    lse_hbm,
    k_hbm,
    v_hbm,
    q_hbm,
    do_hbm,
    x_hbm,
    qg_ref,
    kg_ref,
    vg_ref,
    wg_ref,
    chosen_s,
    lse_s,
    q6,
    do6,
    x_s,
    kw,
    vw,
    kt,
    bias_own,
    bias_out,
    bias_sib,
    own_bias,
    p_s,
    t_s,
    pb_s,
    ds_own,
    ds_sib,
    dv_acc,
    dvo,
    dvi,
    dk_acc,
    dko,
    dki,
    dl_out,
    dl_in,
    dt_out,
    dt_in,
    dq_out,
    dq_in,
    x_t,
    x_in,
    vall,
    late,
    po,
    ri,
    ld_sem,
    q_ld,
    do_ld,
    k_send,
    k_recv,
    v_send,
    v_recv,
    dv_send,
    dv_recv,
    dk_send,
    dk_recv,
    sib_send,
    sib_recv,
    x_send,
    x_recv,
    vg_send,
    vg_recv,
    late_send,
    late_recv,
    rs_send,
    rs_recv,
):
    me = lax.axis_index("kv")
    tp = lax.axis_index("tp")
    core = lax.rem(me, 2)
    chip = me // 2
    sib = me + 1 - 2 * core
    chips = nk // 2
    heads, _, hd = q6.shape[1:]
    tok = kw.shape[1]
    nblk = chosen_s.shape[0]
    blk = tok // nblk
    scale = hd**-0.5
    per_tp, _, rw, _ = x_t.shape
    half = per_tp // 2
    part_rows = half // 2
    f32, bf = jnp.float32, jnp.bfloat16

    barrier = pltpu.get_barrier_semaphore()

    @pl.loop(1, chips)
    def _(j):
        pl.semaphore_signal(
            barrier,
            inc=1,
            device_id=(lax.rem(chip + j, chips) * 2 + core, tp),
            device_id_type=MESH,
        )

    pl.semaphore_signal(barrier, inc=1, device_id=(sib, tp), device_id_type=MESH)
    for dt in range(1, nt):
        for kv in (me, sib):
            pl.semaphore_signal(
                barrier, inc=1, device_id=(kv, lax.rem(tp + dt, nt)), device_id_type=MESH
            )

    load_k, load_v, load_x, load_chosen, load_lse = (
        pltpu.make_async_copy(src, dst, ld_sem.at[i])
        for i, (src, dst) in enumerate(
            (
                (k_hbm, kw.at[0]),
                (v_hbm, vw.at[0]),
                (x_hbm, x_s),
                (chosen_hbm, chosen_s),
                (lse_hbm, lse_s.at[0]),
            )
        )
    )
    load_q = [
        pltpu.make_async_copy(q_hbm.at[:, pl.ds(a * hd, hd)], q6.at[0, a], q_ld.at[a])
        for a in range(heads)
    ]
    load_do = [
        pltpu.make_async_copy(do_hbm.at[:, pl.ds(a * hd, hd)], do6.at[0, a], do_ld.at[a])
        for a in range(heads)
    ]
    for load in (load_k, load_chosen, *load_q, load_lse, load_v, *load_do, load_x):
        load.start()

    def remote(src, dst, send, recv, kv, t=None):
        return pltpu.make_async_remote_copy(
            src_ref=src,
            dst_ref=dst,
            send_sem=send,
            recv_sem=recv,
            device_id=(kv, tp if t is None else t),
            device_id_type=MESH,
        )

    def k_copy(d):
        return remote(kw.at[0], kw.at[d], k_send.at[d], k_recv.at[d], me + 2 * d)

    def v_copy(d):
        return remote(vw.at[0], vw.at[d], v_send.at[d], v_recv.at[d], me + 2 * d)

    def dv_copy(d):
        return remote(dvo.at[d], dvi.at[d], dv_send.at[d], dv_recv.at[d], me - 2 * d)

    def dk_copy(d):
        return remote(dko.at[d], dki.at[d], dk_send.at[d], dk_recv.at[d], me - 2 * d)

    def to_sib(i, src, dst):
        return remote(src, dst, sib_send.at[i], sib_recv.at[i], sib)

    send_q = to_sib(0, q6.at[0], q6.at[1])
    send_lse = to_sib(1, lse_s.at[0], lse_s.at[1])
    send_bias = to_sib(2, bias_out, bias_sib)
    send_do = to_sib(3, do6.at[0], do6.at[1])
    send_x = to_sib(4, x_t.at[:, 1 - core], x_in.at[tp, core])
    send_dl = to_sib(5, dl_out, dl_in)
    send_dt = to_sib(6, dt_out, dt_in)
    send_dq = [
        to_sib(7 + i, dq_out.at[pl.ds(i * heads // 2, heads // 2)], dq_in.at[pl.ds(i * heads // 2, heads // 2)])
        for i in range(2)
    ]

    with scope("barrier_wait"):
        pl.semaphore_wait(barrier, chips + 2 * (nt - 1))

    load_k.wait()
    for d in range(1, SPAN):

        @pl.when(chip + d < chips)
        def _():
            k_copy(d).start()

    for load in load_q:
        load.wait()
    send_q.start()
    load_lse.wait()
    send_lse.start()
    load_v.wait()
    for d in range(1, SPAN):

        @pl.when(chip + d < chips)
        def _():
            v_copy(d).start()

    load_chosen.wait()
    with scope("bias"):
        row = lax.broadcasted_iota(jnp.int32, (nblk, tok), 0)
        pos = lax.broadcasted_iota(jnp.int32, (1, tok), 1)
        lists = []
        for slot in range(chosen_s.shape[2]):
            ids = jnp.full((1, tok), NO_BLOCK, jnp.int32)
            for b in range(nblk):
                block = chosen_s[b, 0, slot]
                block = jnp.where(block < me * nblk + b, block, NO_BLOCK)
                ids = jnp.where(pos >= b * blk, block, ids)
            lists.append(ids)
        lists.append(me * nblk + pos // blk)
        for o in range(REACH + 1):
            ids = row + (me - o) * nblk
            hit = ids == lists[0]
            for other in lists[1:]:
                hit = hit | (ids == other)
            marked = jnp.where(hit, 0.0, MASKED)
            if o % 2:
                bias_out[o // 2] = marked
            else:
                bias_own[o // 2] = marked
        key_row = lax.broadcasted_iota(jnp.int32, (blk, tok), 0)
        query = lax.broadcasted_iota(jnp.int32, (blk, tok), 1)
        for j in range(nblk):
            own_bias[j * blk : (j + 1) * blk, :] = jnp.where(
                key_row + j * blk > query, MASKED, bias_own[0, j : j + 1, :]
            )
    for load in load_do:
        load.wait()
    send_do.start()
    send_bias.start()

    load_x.wait()
    with scope("xT"):
        x_t[...] = x_s[...].T.reshape(x_t.shape)
    early = pl.ds(0, half)
    x_copies = []
    for dt in range(1, nt):
        other = lax.rem(tp + dt, nt)
        for s, kv, par in ((0, me, core), (1, sib, 1 - core)):
            x_copies.append(
                remote(
                    x_t.at[early, par],
                    x_in.at[tp, core, early],
                    x_send.at[dt, s],
                    x_recv.at[tp, core],
                    kv,
                    other,
                )
            )
    for copy in x_copies:
        copy.start()
    send_x.start()

    zero = jnp.zeros((tok, hd), bf)
    for d in range(1, SPAN):

        @pl.when(chip < d)
        def _():
            kw[d] = zero
            vw[d] = zero

        @pl.when(chip + d >= chips)
        def _():
            dvi[d] = zero
            dki[d] = zero

    def weights(whose, slot, d, bias, buf):
        keys = kw[d]
        for a in range(heads):
            s = lax.dot_general(keys, q6[whose, a], NT, preferred_element_type=f32)
            s = s * (scale * LOG2E)
            lse = lse_s[whose, a : a + 1, :] * LOG2E
            if bias is None:
                p = jnp.exp2(s + (own_bias[...] - lse))
            else:
                p = jnp.exp2(s.reshape(nblk, blk, tok) + (bias - lse)[:, None, :]).reshape(tok, tok)
            p_s[a, slot] = p
            pb_s[buf, :, a * tok : (a + 1) * tok] = p.astype(bf)
        return jnp.dot(
            pb_s[buf], do6[whose].reshape(heads * tok, hd), preferred_element_type=f32
        )

    with scope("tile0"):
        dv_acc[0] = weights(0, 0, 0, None, 0)

    with scope("k1_wait"):

        @pl.when(chip >= 1)
        def _():
            k_copy(1).wait_recv()

    with scope("own1"):
        own_part = weights(0, 1, 1, bias_own[1], 1)
    with scope("q_wait"):
        send_q.wait_recv()
        send_lse.wait_recv()
        send_bias.wait_recv()
        send_do.wait_recv()
    with scope("sib1"):
        near = 1 - core
        dvo[1] = (own_part + weights(1, SPAN + near, 1, bias_sib[near], 0)).astype(bf)

    @pl.when(chip >= 1)
    def _():
        dv_copy(1).start()

    with scope("k2_wait"):

        @pl.when(chip >= 2)
        def _():
            k_copy(2).wait_recv()

    with scope("tile2"):
        dv_acc[1] = weights(0, 2, 2, bias_own[2], 1)
        dv_acc[2] = weights(1, SPAN + core, 2 * core, bias_sib[core], 0)
        dvo[2] = (dv_acc[1] + jnp.where(core == 1, dv_acc[2], 0.0)).astype(bf)

    @pl.when(chip >= 2)
    def _():
        dv_copy(2).start()

    for d in range(SPAN):
        kt[d] = kw[d].T

    with scope("v_wait"):
        for d in range(1, SPAN):

            @pl.when(chip >= d)
            def _():
                v_copy(d).wait_recv()

    with scope("sib_gw"):
        for a in range(heads):
            gw = lax.dot_general(
                vw[pl.ds(core, 2)].reshape(2 * tok, hd), do6[1, a], NT, preferred_element_type=f32
            )
            t = p_s[a, SPAN:].reshape(2 * tok, tok) * gw
            t_s[a] = t
            dl_out[a : a + 1, :] = jnp.sum(t, 0, keepdims=True)
    send_dl.start()

    with scope("dv_wait"):
        for d in range(1, SPAN):

            @pl.when(chip + d < chips)
            def _():
                dv_copy(d).wait_recv()

    value = dv_acc[0] + jnp.where(core == 0, dv_acc[2], 0.0)
    for d in range(1, SPAN):
        value = value + dvi[d].astype(f32)
    value = value.astype(bf)
    vg_ref[...] = value
    vall[tp, core] = value
    vg_copies = [remote(vall.at[tp, core], vall.at[tp, core], vg_send.at[0, 1], vg_recv.at[tp, core], sib)]
    for dt in range(1, nt):
        other = lax.rem(tp + dt, nt)
        for s, kv in ((0, me), (1, sib)):
            vg_copies.append(
                remote(
                    vall.at[tp, core],
                    vall.at[tp, core],
                    vg_send.at[dt, s],
                    vg_recv.at[tp, core],
                    kv,
                    other,
                )
            )
    for copy in vg_copies:
        copy.start()

    def score_grad(a):
        gw = lax.dot_general(
            vw[...].reshape(SPAN * tok, hd), do6[0, a], NT, preferred_element_type=f32
        )
        p = p_s[a, :SPAN].reshape(SPAN * tok, tok)
        own = jnp.sum(p * gw, 0, keepdims=True)
        dt_out[a : a + 1, :] = own
        delta = own + dl_in[a : a + 1, :]
        ds_own[:, a * tok : (a + 1) * tok] = (p * (gw - delta)).astype(bf)

    with scope("dl_wait"):
        send_dl.wait_recv()
    split = heads // 2
    with scope("own_ds_a"):
        for a in range(split):
            score_grad(a)

    def rs_copy(to):
        return remote(po.at[to], ri.at[chip], rs_send.at[to], rs_recv.at[chip], to * 2 + core)

    def vg_wait(t, c):
        remote(vall.at[t, c], vall.at[t, c], vg_send.at[0, 0], vg_recv.at[t, c], sib).wait_recv()

    def send_rows(start, count):
        @pl.loop(0, count)
        def _(j):
            @pl.when(start + j != chip)
            def _():
                rs_copy(start + j).start()

    with scope("vg_wait"):
        vg_wait(tp, 1 - core)
        send_x.wait_recv()

    def own_rows(first, count, t):
        rows = pl.ds(first, count)
        return jnp.dot(
            x_t[rows, core].reshape(count * rw, tok), vall[t, core], preferred_element_type=f32
        ) + jnp.dot(
            x_in[tp, 1 - core, rows].reshape(count * rw, tok),
            vall[t, 1 - core],
            preferred_element_type=f32,
        )

    with scope("w_own"):
        for h in range(2):
            start = tp * per_tp + h * half
            po[pl.ds(start, half)] = own_rows(h * half, half, tp).astype(bf).reshape(half, rw, hd)
            send_rows(start, half)
    for dt in range(1, nt):
        t = lax.rem(tp + dt, nt)
        with scope("x_wait"):
            for c in range(2):
                remote(
                    x_t.at[early, 0], x_in.at[t, c, early], x_send.at[0, 0], x_recv.at[t, c], sib
                ).wait_recv()
        with scope("w_early"):
            start = t * per_tp
            po[pl.ds(start, half)] = (
                (
                    jnp.dot(
                        x_in[t, 0, early].reshape(half * rw, tok),
                        vall[tp, 0],
                        preferred_element_type=f32,
                    )
                    + jnp.dot(
                        x_in[t, 1, early].reshape(half * rw, tok),
                        vall[tp, 1],
                        preferred_element_type=f32,
                    )
                )
                .astype(bf)
                .reshape(half, rw, hd)
            )
            send_rows(start, half)

    with scope("own_ds_b"):
        for a in range(split, heads):
            score_grad(a)
    send_dt.start()

    def late_copy(dt, i):
        other = lax.rem(tp + dt, nt)
        rows = pl.ds(tp * per_tp + half + i * part_rows, part_rows)
        return remote(
            late.at[dt, pl.ds(i * part_rows, part_rows)],
            po.at[rows],
            late_send.at[dt, i],
            late_recv.at[tp, i],
            me,
            other,
        )

    for dt in range(1, nt):
        t = lax.rem(tp + dt, nt)
        with scope("vg_other_wait"):
            vg_wait(t, 0)
            vg_wait(t, 1)
        with scope("w_late"):
            late[dt] = own_rows(half, half, t).astype(bf).reshape(half, rw, hd)
            for i in range(2):
                late_copy(dt, i).start()

    def forward(i):
        for dt in range(1, nt):
            t = lax.rem(tp + dt, nt)
            start = t * per_tp + half + i * part_rows
            rows = pl.ds(start, part_rows)
            with scope("late_wait"):
                remote(
                    po.at[rows], po.at[rows], late_send.at[0, 0], late_recv.at[t, i], me, t
                ).wait_recv()
            send_rows(start, part_rows)

    def dk_part(ds, d, whose):
        return jnp.dot(
            ds[d * tok : (d + 1) * tok, :],
            q6[whose].reshape(heads * tok, hd),
            preferred_element_type=f32,
        )

    with scope("dk_own"):
        for d in range(1, SPAN):
            dk_acc[d] = dk_part(ds_own, d, 0)

    with scope("dt_wait"):
        send_dt.wait_recv()
    with scope("sib_ds"):
        for a in range(heads):
            delta = dl_out[a : a + 1, :] + dt_in[a : a + 1, :]
            ds_sib[:, a * tok : (a + 1) * tok] = (
                t_s[a] - p_s[a, SPAN:].reshape(2 * tok, tok) * delta
            ).astype(bf)
    with scope("dk_sib"):
        dk_acc[0] = jnp.zeros((tok, hd), f32)
        for s in range(2):
            d = core + s
            dk_acc[d] = dk_acc[d] + dk_part(ds_sib, s, 1)
        for d in range(1, SPAN):
            dko[d] = (dk_acc[d] * scale).astype(bf)
    for d in range(1, SPAN):

        @pl.when(chip >= d)
        def _():
            dk_copy(d).start()

    forward(0)
    with scope("dq_sib"):
        for i in range(2):
            for a in range(i * split, (i + 1) * split):
                dq = jnp.dot(
                    kt[core], ds_sib[:tok, a * tok : (a + 1) * tok], preferred_element_type=f32
                ) + jnp.dot(
                    kt[core + 1], ds_sib[tok:, a * tok : (a + 1) * tok], preferred_element_type=f32
                )
                dq_out[a] = (dq * scale).astype(bf)
            send_dq[i].start()
    forward(1)

    with scope("dk0"):
        key = (dk_acc[0] + dk_part(ds_own, 0, 0)) * scale

    with scope("dq_own"):
        for i in range(2):
            send_dq[i].wait_recv()
            for a in range(i * split, (i + 1) * split):
                dq = sum(
                    jnp.dot(
                        kt[d],
                        ds_own[d * tok : (d + 1) * tok, a * tok : (a + 1) * tok],
                        preferred_element_type=f32,
                    )
                    for d in range(SPAN)
                )
                dq = dq * scale + dq_in[a].astype(f32)
                qg_ref[:, a * hd : (a + 1) * hd] = dq.T.astype(bf)

    with scope("dk_wait"):
        for d in range(1, SPAN):

            @pl.when(chip + d < chips)
            def _():
                dk_copy(d).wait_recv()

            key = key + dki[d].astype(f32)
        kg_ref[...] = key.astype(bf)

    ri[pl.ds(chip, 1)] = po[pl.ds(chip, 1)]

    with scope("rs_wait"):

        @pl.loop(1, chips)
        def _(j):
            src = lax.rem(chip + j, chips)
            remote(
                po.at[src], ri.at[src], rs_send.at[src], rs_recv.at[src], src * 2 + core
            ).wait_recv()

    wg_ref[...] = jnp.sum(ri[...].astype(f32), 0)

    with scope("send_wait"):
        for d in range(1, SPAN):

            @pl.when(chip + d < chips)
            def _():
                k_copy(d).wait_send()
                v_copy(d).wait_send()

            @pl.when(chip >= d)
            def _():
                dv_copy(d).wait_send()
                dk_copy(d).wait_send()

        for copy in (
            send_q,
            send_lse,
            send_bias,
            send_do,
            send_x,
            send_dl,
            send_dt,
            *send_dq,
            *x_copies,
            *vg_copies,
        ):
            copy.wait_send()
        for dt in range(1, nt):
            for i in range(2):
                late_copy(dt, i).wait_send()

        @pl.loop(1, chips)
        def _(j):
            rs_copy(lax.rem(chip + j, chips)).wait_send()


def finish(*refs):
    count = len(refs) // 2
    sems = refs[-1]
    copies = [
        pltpu.make_async_copy(refs[i], refs[count + i], sems.at[i]) for i in range(count)
    ]
    for copy in copies:
        copy.start()
    for copy in copies:
        copy.wait()


def shards(nk, nt, queries, keys, values, log_sums, out_grad, chosen, inputs):
    tok, hd = keys.shape
    heads = queries.shape[1] // hd
    nblk = chosen.shape[0]
    feats = inputs.shape[1]
    rw = feats * nt // nk
    per_tp = feats // (2 * rw)
    bf, f32 = jnp.bfloat16, jnp.float32
    dma = pltpu.SemaphoreType.DMA
    vmem = pl.BlockSpec(memory_space=pltpu.VMEM)
    hbm = pl.BlockSpec(memory_space=pl.ANY)
    chips = nk // 2
    parts = pl.pallas_call(
        functools.partial(kernel, nk, nt),
        out_shape=(
            jax.ShapeDtypeStruct((tok, heads * hd), bf),
            jax.ShapeDtypeStruct((tok, hd), bf),
            jax.ShapeDtypeStruct((tok, hd), bf),
            jax.ShapeDtypeStruct((rw, hd), f32),
        ),
        in_specs=[hbm] * 7,
        out_specs=(vmem, vmem, vmem, vmem),
        scratch_shapes=[
            pltpu.SMEM(chosen.shape, jnp.int32),
            pltpu.VMEM((2, heads, tok), f32),
            pltpu.VMEM((2, heads, tok, hd), bf),
            pltpu.VMEM((2, heads, tok, hd), bf),
            pltpu.VMEM((tok, feats), bf),
            pltpu.VMEM((SPAN, tok, hd), bf),
            pltpu.VMEM((SPAN, tok, hd), bf),
            pltpu.VMEM((SPAN, hd, tok), bf),
            pltpu.VMEM((SPAN, nblk, tok), f32),
            pltpu.VMEM((2, nblk, tok), f32),
            pltpu.VMEM((2, nblk, tok), f32),
            pltpu.VMEM((tok, tok), f32),
            pltpu.VMEM((heads, SPAN + 2, tok, tok), f32),
            pltpu.VMEM((heads, 2 * tok, tok), f32),
            pltpu.VMEM((2, tok, heads * tok), bf),
            pltpu.VMEM((SPAN * tok, heads * tok), bf),
            pltpu.VMEM((2 * tok, heads * tok), bf),
            pltpu.VMEM((SPAN, tok, hd), f32),
            pltpu.VMEM((SPAN, tok, hd), bf),
            pltpu.VMEM((SPAN, tok, hd), bf),
            pltpu.VMEM((SPAN, tok, hd), f32),
            pltpu.VMEM((SPAN, tok, hd), bf),
            pltpu.VMEM((SPAN, tok, hd), bf),
            pltpu.VMEM((heads, tok), f32),
            pltpu.VMEM((heads, tok), f32),
            pltpu.VMEM((heads, tok), f32),
            pltpu.VMEM((heads, tok), f32),
            pltpu.VMEM((heads, hd, tok), bf),
            pltpu.VMEM((heads, hd, tok), bf),
            pltpu.VMEM((per_tp, 2, rw, tok), bf),
            pltpu.VMEM((nt, 2, per_tp, rw, tok), bf),
            pltpu.VMEM((nt, 2, tok, hd), bf),
            pltpu.VMEM((nt, per_tp // 2, rw, hd), bf),
            pltpu.VMEM((chips, rw, hd), bf),
            pltpu.VMEM((chips, rw, hd), bf),
            dma((5,)),
            dma((heads,)),
            dma((heads,)),
            dma((SPAN,)),
            dma((SPAN,)),
            dma((SPAN,)),
            dma((SPAN,)),
            dma((SPAN,)),
            dma((SPAN,)),
            dma((SPAN,)),
            dma((SPAN,)),
            dma((9,)),
            dma((9,)),
            dma((nt, 2)),
            dma((nt, 2)),
            dma((nt, 2)),
            dma((nt, 2)),
            dma((nt, 2)),
            dma((nt, 2)),
            dma((chips,)),
            dma((chips,)),
        ],
        compiler_params=pltpu.CompilerParams(
            collective_id=0, has_side_effects=True, vmem_limit_bytes=60 * 1024 * 1024
        ),
    )(chosen, log_sums, keys, values, queries, out_grad, inputs)
    return pl.pallas_call(
        finish,
        out_shape=tuple(jax.ShapeDtypeStruct(part.shape, part.dtype) for part in parts),
        in_specs=[vmem] * len(parts),
        out_specs=(hbm,) * len(parts),
        scratch_shapes=[dma((len(parts),))],
    )(*parts)


def solution(mesh):
    in_specs = (
        P("kv", "tp"),
        P("kv", "tp"),
        P("kv", "tp"),
        P("tp", "kv"),
        P("kv", "tp"),
        P("kv", "tp", None),
        P("kv", "tp"),
    )
    out_specs = (P("kv", "tp"), P("kv", "tp"), P("kv", "tp"), P("kv", "tp"))
    return jax.shard_map(
        functools.partial(shards, mesh.shape["kv"], mesh.shape["tp"]),
        mesh=mesh,
        in_specs=in_specs,
        out_specs=out_specs,
        check_vma=False,
    )
```

time: 37.7 us -> 32.8 us (0.87); the launches traced: 37 us -> 32.5 us
  Pallas kernels: 36.4 us -> 31.9 us
    pallas_call x1, Pallas kernels: 34.5 us -> 29.9 us  [shards(): pl.pallas_call(functools.partial(kernel, nk, nt), out_shape=(jax.ShapeDty...]
where the time goes in v1:
time: 32.8 us; the launch traced here: 32.5 us
  Pallas kernels  31.9 us (97%)
  between operations  0.64 us (2%)
    pallas_call x1, Pallas kernels, shards(): pl.pallas_call(functools.partial(kernel, nk, nt), out_shape=(jax.ShapeDty...  29.9 us
    pallas_call x1, Pallas kernels, shards(): pl.pallas_call(finish, out_shape=tuple((jax.ShapeDtypeStruct(part.shape,...  1.93 us

profile of v1, /device:TPU:14, one launch (start us, length us, event | category | flops | bytes accessed | tf_op | source)
XLA Modules:
  0.0 32.5 jit_solution(13216354167040779841)
XLA Ops:
  0.6 29.9 %shard_map.102 = (bf16[256,768]{1,0:T(8,128)(2,1)}, bf16[256,128]{1,0:T(8,128)(2,1)}, bf16[256,128]{1,0:T(8,128)(2,1)}, f32[192,128]{1,0:T(8,128)}) custom-call(s32[4,1,8]{2,1,0:T(1,128)} %chosen_hbm.1, f32[6,256]{1,0:T(8,128)} %lse_hbm.1, bf16[256,128]{1,0:T(8,128)(2,1)} %k_hbm.1, bf16[256,128]{1,0:T(8,128)(2,1)} %v_hbm.1, bf16[256,768]{1,0:T(8,128)(2,1)} %q_hbm.1, ...), custom_call_target="tpu_custom_call" | custom-call | tf_op jit(solution)/shard_map/pallas_call | solution.py:641
  30.6 1.9 %shard_map.103 = (bf16[256,768]{1,0:T(8,128)(2,1)}, bf16[256,128]{1,0:T(8,128)(2,1)}, bf16[256,128]{1,0:T(8,128)(2,1)}, f32[192,128]{1,0:T(8,128)}) custom-call(bf16[256,768]{1,0:T(8,128)(2,1)} %get-tuple-element.8.refs_0_, bf16[256,128]{1,0:T(8,128)(2,1)} %get-tuple-element.9.refs_1_, bf16[256,128]{1,0:T(8,128)(2,1)} %get-tuple-element.10.refs_2_, ...), custom_call_target="tpu_custom_call" | custom-call | tf_op jit(solution)/shard_map/pallas_call | solution.py:713

commit v2 on v1

v2 whole, which is shorter than its diff:
```python
import functools

import jax
import jax.numpy as jnp
from jax import lax
from jax.experimental import pallas as pl
from jax.experimental.pallas import tpu as pltpu
from jax.sharding import PartitionSpec as P

REACH = 4
BACK = REACH // 2
SPAN = BACK + 1
STEPS = tuple(step for d in range(1, BACK + 1) for step in (d, -d))
LAST = 3
MASKED = -1e30
NO_BLOCK = -(1 << 20)
LOG2E = 1.4426950408889634
MESH = pl.DeviceIdType.MESH
NT = (((1,), (1,)), ((), ()))
scope = jax.named_scope


def kernel(
    nk,
    nt,
    chosen_hbm,
    lse_hbm,
    k_hbm,
    v_hbm,
    q_hbm,
    do_hbm,
    x_hbm,
    qg_ref,
    kg_ref,
    vg_ref,
    wg_ref,
    chosen_s,
    lse_s,
    q6,
    do6,
    x_s,
    kvw,
    kt,
    bias_own,
    bias_out,
    bias_sib,
    own_bias,
    p_s,
    t_s,
    pb_s,
    ds_own,
    ds_sib,
    dv_own,
    dv_far,
    dk_acc,
    back_out,
    back_in,
    dl_out,
    dl_in,
    dt_out,
    dt_in,
    dq_out,
    dq_in,
    x_t,
    x_in,
    vall,
    late,
    late_in,
    pf,
    po,
    yi,
    zo,
    ri,
    ld_sem,
    kv_send,
    k_recv,
    v_recv,
    back_send,
    dv_recv,
    dk_recv,
    sib_send,
    sib_recv,
    x_send,
    x_recv,
    vg_send,
    vg_recv,
    late_send,
    late_recv,
    y_send,
    y_recv,
    rs_send,
    rs_recv,
    go_sem,
):
    me = lax.axis_index("kv")
    tp = lax.axis_index("tp")
    core = lax.rem(me, 2)
    chip = me // 2
    sib = me + 1 - 2 * core
    side = lax.rem(chip, 2)
    across = me + 2 - 4 * side
    chips = nk // 2
    _, heads, tok, hd = q6.shape
    kw, vw = kvw.at[0], kvw.at[1]
    dvo, dko = back_out.at[0], back_out.at[1]
    dvi, dki = back_in.at[0], back_in.at[1]
    nblk = chosen_s.shape[0]
    blk = tok // nblk
    scale = hd**-0.5
    per_tp, _, rw, _ = x_t.shape
    half = per_tp // 2
    pairs = chips // 2
    hh = half // 2
    mine = chip // 2
    half_heads = heads // 2
    mid = 1 - lax.rem(tp, 2)
    f32, bf = jnp.float32, jnp.bfloat16

    behind = chip
    ahead = chips - 1 - chip
    near_chips = [(step, ahead >= step if step > 0 else behind >= -step) for step in STEPS]
    barrier = pltpu.get_barrier_semaphore()
    count = 1 + 3 * (nt - 1)
    for step, exists in near_chips:
        count = count + jnp.where(exists, 1, 0)

        @pl.when(exists)
        def _():
            pl.semaphore_signal(
                barrier, inc=1, device_id=(me + 2 * step, tp), device_id_type=MESH
            )

    pl.semaphore_signal(barrier, inc=1, device_id=(sib, tp), device_id_type=MESH)
    for dt in range(1, nt):
        for kv in (me, sib, across):
            pl.semaphore_signal(
                barrier, inc=1, device_id=(kv, lax.rem(tp + dt, nt)), device_id_type=MESH
            )

    load_k, load_v, load_x, load_chosen, load_lse = (
        pltpu.make_async_copy(src, dst, ld_sem.at[i])
        for i, (src, dst) in enumerate(
            (
                (k_hbm, kw.at[0]),
                (v_hbm, vw.at[0]),
                (x_hbm, x_s),
                (chosen_hbm, chosen_s),
                (lse_hbm, lse_s.at[0]),
            )
        )
    )
    load_q, load_do = (
        [
            pltpu.make_async_copy(src.at[:, pl.ds(a * hd, hd)], dst.at[0, a], ld_sem.at[i])
            for a in range(heads)
        ]
        for i, src, dst in ((5, q_hbm, q6), (6, do_hbm, do6))
    )

    def all_of(ref, sem):
        return pltpu.make_async_copy(ref, ref, sem)

    for load in (load_k, load_chosen, *load_q, load_lse, load_v, *load_do, load_x):
        load.start()

    def remote(src, dst, send, recv, kv, t=None):
        return pltpu.make_async_remote_copy(
            src_ref=src,
            dst_ref=dst,
            send_sem=send,
            recv_sem=recv,
            device_id=(kv, tp if t is None else t),
            device_id_type=MESH,
        )

    def k_copy(d):
        return remote(kw.at[0], kw.at[d], kv_send, k_recv.at[d - 1], me + 2 * d)

    def v_copy(d):
        return remote(vw.at[0], vw.at[d], kv_send, v_recv, me + 2 * d)

    def dv_copy(d):
        return remote(dvo.at[d - 1], dvi.at[d - 1], back_send, dv_recv, me - 2 * d)

    def dk_copy(d):
        return remote(dko.at[d - 1], dki.at[d - 1], back_send, dk_recv, me - 2 * d)

    def each_count(left, wait):
        for count in range(1, BACK + 1):
            here = (left == count) if count < BACK else (left >= count)

            @pl.when(here)
            def _():
                wait(pl.ds(0, count))

    def to_sib(i, j, src, dst):
        return remote(src, dst, sib_send.at[i], sib_recv.at[j], sib)

    send_q = to_sib(0, 0, q6.at[0], q6.at[1])
    send_do = to_sib(0, 0, do6.at[0], do6.at[1])
    send_lse = to_sib(1, 1, lse_s.at[0], lse_s.at[1])
    send_bias = to_sib(2, 2, bias_out, bias_sib)
    send_x = to_sib(3, 3, x_t.at[:, 1 - core], x_in.at[tp, core])
    send_dl = to_sib(4, 4, dl_out, dl_in)
    send_dt = to_sib(4, 5, dt_out, dt_in)
    send_dq = [
        to_sib(5, 6 + i, dq_out.at[pl.ds(i * half_heads, half_heads)], dq_in.at[pl.ds(i * half_heads, half_heads)])
        for i in range(2)
    ]

    with scope("barrier_wait"):
        pl.semaphore_wait(barrier, count)

    def relay(point):
        for i, step, left, done in ((0, -BACK, ahead, behind), (1, BACK, behind, ahead)):
            hops = left // BACK
            turn = hops == point if point < LAST else hops >= point

            @pl.when(turn & (hops > 0))
            def _():
                pl.semaphore_wait(go_sem.at[i], 1)

            @pl.when(turn & (done >= BACK))
            def _():
                pl.semaphore_signal(
                    go_sem.at[i], inc=1, device_id=(me + 2 * step, tp), device_id_type=MESH
                )

    load_k.wait()
    for d in range(1, SPAN):

        @pl.when(chip + d < chips)
        def _():
            k_copy(d).start()

    relay(0)
    all_of(q6.at[0], ld_sem.at[5]).wait()
    send_q.start()
    load_lse.wait()
    send_lse.start()
    load_v.wait()
    for d in range(1, SPAN):

        @pl.when(chip + d < chips)
        def _():
            v_copy(d).start()

    load_chosen.wait()
    with scope("bias"):
        row = lax.broadcasted_iota(jnp.int32, (nblk, tok), 0)
        pos = lax.broadcasted_iota(jnp.int32, (1, tok), 1)
        lists = []
        for slot in range(chosen_s.shape[2]):
            ids = jnp.full((1, tok), NO_BLOCK, jnp.int32)
            for b in range(nblk):
                block = chosen_s[b, 0, slot]
                block = jnp.where(block < me * nblk + b, block, NO_BLOCK)
                ids = jnp.where(pos >= b * blk, block, ids)
            lists.append(ids)
        lists.append(me * nblk + pos // blk)
        for o in range(REACH + 1):
            ids = row + (me - o) * nblk
            hit = ids == lists[0]
            for other in lists[1:]:
                hit = hit | (ids == other)
            marked = jnp.where(hit, 0.0, MASKED)
            if o % 2:
                bias_out[o // 2] = marked
            else:
                bias_own[o // 2] = marked
        key_row = lax.broadcasted_iota(jnp.int32, (blk, tok), 0)
        query = lax.broadcasted_iota(jnp.int32, (blk, tok), 1)
        for j in range(nblk):
            own_bias[j * blk : (j + 1) * blk, :] = jnp.where(
                key_row + j * blk > query, MASKED, bias_own[0, j : j + 1, :]
            )
    all_of(do6.at[0], ld_sem.at[6]).wait()
    send_do.start()
    send_bias.start()

    load_x.wait()
    with scope("xT"):
        x_t[...] = x_s[...].T.reshape(x_t.shape)

    def end_rows(t):
        return pl.ds(lax.rem(t, 2) * half, half)

    early = end_rows(tp)
    x_copies = []
    for dt in range(1, nt):
        other = lax.rem(tp + dt, nt)
        for s, kv, par in ((0, me, core), (1, sib, 1 - core)):
            x_copies.append(
                remote(
                    x_t.at[early, par],
                    x_in.at[tp, core, early],
                    x_send.at[dt - 1],
                    x_recv.at[nt - dt - 1],
                    kv,
                    other,
                )
            )
    for copy in x_copies:
        copy.start()

    zero = jnp.zeros((tok, hd), bf)
    for d in range(1, SPAN):

        @pl.when(chip < d)
        def _():
            kw[d] = zero
            vw[d] = zero

        @pl.when(chip + d >= chips)
        def _():
            dvi[d - 1] = zero
            dki[d - 1] = zero

    def weights(whose, slot, d, bias, buf):
        keys = kw[d]
        for a in range(heads):
            s = lax.dot_general(keys, q6[whose, a], NT, preferred_element_type=f32)
            s = s * (scale * LOG2E)
            lse = lse_s[whose, a : a + 1, :] * LOG2E
            if bias is None:
                p = jnp.exp2(s + (own_bias[...] - lse))
            else:
                p = jnp.exp2(s.reshape(nblk, blk, tok) + (bias - lse)[:, None, :]).reshape(tok, tok)
            p_s[a, slot] = p
            pb_s[buf, :, a * tok : (a + 1) * tok] = p.astype(bf)
        return jnp.dot(
            pb_s[buf], do6[whose].reshape(heads * tok, hd), preferred_element_type=f32
        )

    near = 1 - core
    far = 2 * core

    def far_tile():
        dv_far[...] = weights(1, SPAN + 1, far, bias_sib[core], 0)

    with scope("tile0"):
        dv_own[...] = weights(0, 0, 0, None, 0)

    with scope("q_wait"):
        all_of(q6, sib_recv.at[0]).wait()
        send_lse.wait_recv()
        send_bias.wait_recv()

    relay(1)

    @pl.when(core == 0)
    def _():
        with scope("far0"):
            far_tile()

    def tile1():
        with scope("k1_wait"):

            @pl.when(chip >= 1)
            def _():
                k_copy(1).wait_recv()

        with scope("d1"):
            dvo[0] = (
                weights(0, 1, 1, bias_own[1], 1) + weights(1, SPAN, 1, bias_sib[near], 0)
            ).astype(bf)

        @pl.when(chip >= 1)
        def _():
            dv_copy(1).start()

    def tile2():
        with scope("k2_wait"):

            @pl.when(chip >= 2)
            def _():
                k_copy(2).wait_recv()

        @pl.when(core == 1)
        def _():
            with scope("far1"):
                far_tile()

        with scope("d2"):
            dvo[1] = (
                weights(0, 2, 2, bias_own[2], 1) + jnp.where(core == 1, dv_far[...], 0.0)
            ).astype(bf)

        @pl.when(chip >= 2)
        def _():
            dv_copy(2).start()

    @pl.when(side == 0)
    def _():
        tile2()
        tile1()

    @pl.when(side == 1)
    def _():
        tile1()
        tile2()

    send_x.start()
    relay(2)
    for d in range(SPAN):
        kt[d] = kw[d].T

    with scope("v_wait"):
        each_count(behind, lambda rows: all_of(vw.at[rows], v_recv).wait())

    with scope("sib_gw"):
        for a in range(heads):
            total = jnp.zeros((1, tok), f32)
            for i, d in enumerate((1, far)):
                gw = lax.dot_general(vw[d], do6[1, a], NT, preferred_element_type=f32)
                t = p_s[a, SPAN + i] * gw
                t_s[a, i] = t
                total = total + jnp.sum(t, 0, keepdims=True)
            dl_out[a : a + 1, :] = total
    send_dl.start()

    with scope("dv_wait"):
        each_count(ahead, lambda rows: all_of(dvi.at[rows], dv_recv).wait())

    value = dv_own[...] + jnp.where(core == 0, dv_far[...], 0.0)
    for d in range(1, SPAN):
        value = value + dvi[d - 1].astype(f32)
    value = value.astype(bf)
    vg_ref[...] = value
    vall[tp * 2 + core] = value
    my_vg = vall.at[tp * 2 + core]
    vg_copies = [remote(my_vg, my_vg, vg_send, vg_recv.at[tp * 2 + core], sib)]
    for dt in range(1, nt):
        for kv in (me, sib):
            vg_copies.append(
                remote(my_vg, my_vg, vg_send, vg_recv.at[tp * 2 + core], kv, lax.rem(tp + dt, nt))
            )
    for copy in vg_copies:
        copy.start()

    def score_grad(a):
        gw = lax.dot_general(
            vw[...].reshape(SPAN * tok, hd), do6[0, a], NT, preferred_element_type=f32
        )
        p = p_s[a, :SPAN].reshape(SPAN * tok, tok)
        own = jnp.sum(p * gw, 0, keepdims=True)
        dt_out[a : a + 1, :] = own
        delta = own + dl_in[a : a + 1, :]
        ds_own[:, a * tok : (a + 1) * tok] = (p * (gw - delta)).astype(bf)

    with scope("dl_wait"):
        send_dl.wait_recv()
    split = heads // 2
    with scope("own_ds_a"):
        for a in range(split):
            score_grad(a)

    def rs_copy(m):
        return remote(zo.at[m], ri.at[mine], rs_send, rs_recv, (2 * m + side) * 2 + core)

    def vg_wait(t, c):
        all_of(vall.at[t * 2 + c], vg_recv.at[t * 2 + c]).wait()

    def y_copy(g, first):
        rows = pl.ds(first // 2, hh)
        return remote(po.at[rows, 1 - side], yi.at[rows], y_send, y_recv.at[g], across)

    def put_rows(g, first, part):
        rows = pl.ds(first // 2, hh)
        pf[rows] = part.reshape(hh, 2, rw, hd)
        po[rows] = part.astype(bf).reshape(hh, 2, rw, hd)
        y_copy(g, first).start()

    def pass_rows(first):
        @pl.loop(0, hh)
        def _(j):
            @pl.when(first // 2 + j != mine)
            def _():
                rs_copy(first // 2 + j).start()

    def join_rows(g, first):
        with scope(f"y_wait{g}"):
            y_copy(g, first).wait_recv()
        rows = pl.ds(first // 2, hh)
        zo[rows] = (pf[rows, side] + yi[rows].astype(f32)).astype(bf)
        pass_rows(first)

    with scope("vg_wait"):
        vg_wait(tp, 1 - core)
        send_x.wait_recv()

    def own_rows(first, t):
        rows = pl.ds(first, half)
        return jnp.dot(
            x_t[rows, core].reshape(half * rw, tok), vall[t * 2 + core], preferred_element_type=f32
        ) + jnp.dot(
            x_in[tp, 1 - core, rows].reshape(half * rw, tok),
            vall[t * 2 + 1 - core],
            preferred_element_type=f32,
        )

    with scope("relay"):
        relay(LAST)
    groups = []
    with scope("w_end"):
        first = tp * per_tp + (1 - mid) * half
        put_rows(0, first, own_rows((1 - mid) * half, tp))
        groups.append((0, first))
    with scope("w_mid"):
        first = tp * per_tp + mid * half
        put_rows(nt, first, own_rows(mid * half, tp))
        groups.append((nt, first))

    with scope("own_ds_b"):
        for a in range(split, heads):
            score_grad(a)
    send_dt.start()

    def dk_part(ds, d, whose):
        return jnp.dot(
            ds[d * tok : (d + 1) * tok, :],
            q6[whose].reshape(heads * tok, hd),
            preferred_element_type=f32,
        )

    with scope("dk_own"):
        for d in range(1, SPAN):
            dk_acc[d - 1] = dk_part(ds_own, d, 0)

    for dt in range(1, nt):
        t = lax.rem(tp + dt, nt)
        rows = end_rows(t)
        with scope("x_wait"):
            all_of(x_in.at[t, :, rows], x_recv.at[dt - 1]).wait()
        with scope("w_early"):
            part = sum(
                jnp.dot(
                    x_in[t, c, rows].reshape(half * rw, tok),
                    vall[tp * 2 + c],
                    preferred_element_type=f32,
                )
                for c in range(2)
            )
            first = t * per_tp + lax.rem(t, 2) * half
            put_rows(dt, first, part)
            groups.append((dt, first))

    with scope("dt_wait"):
        send_dt.wait_recv()
    with scope("sib_ds"):
        for a in range(heads):
            delta = dl_out[a : a + 1, :] + dt_in[a : a + 1, :]
            for i in range(2):
                ds_sib[i * tok : (i + 1) * tok, a * tok : (a + 1) * tok] = (
                    t_s[a, i] - p_s[a, SPAN + i] * delta
                ).astype(bf)
    with scope("dk_sib"):
        dko[0] = ((dk_acc[0] + dk_part(ds_sib, 0, 1)) * scale).astype(bf)
        dk_far = dk_part(ds_sib, 1, 1)
        dko[1] = ((dk_acc[1] + jnp.where(core == 1, dk_far, 0.0)) * scale).astype(bf)
        dk_acc[0] = jnp.where(core == 0, dk_far, 0.0)
    for d in range(1, SPAN):

        @pl.when(chip >= d)
        def _():
            dk_copy(d).start()

    def late_copy(dt, i):
        return remote(
            late.at[dt - 1, :, side if i == 0 else 1 - side],
            late_in.at[tp, side],
            late_send,
            late_recv.at[nt - dt - 1],
            me if i == 0 else across,
            lax.rem(tp + dt, nt),
        )

    for dt in range(1, nt):
        t = lax.rem(tp + dt, nt)
        with scope("vg_other_wait"):
            vg_wait(t, 0)
            vg_wait(t, 1)
        with scope("w_late"):
            late[dt - 1] = own_rows(mid * half, t).astype(bf).reshape(hh, 2, rw, hd)
            for i in (1, 0):
                late_copy(dt, i).start()

    def join_late():
        for dt in range(1, nt):
            t = lax.rem(tp + dt, nt)
            first = t * per_tp + (1 - lax.rem(t, 2)) * half
            with scope("late_wait"):
                all_of(late_in.at[t], late_recv.at[dt - 1]).wait()
            zo[pl.ds(first // 2, hh)] = (
                late_in[t, 0].astype(f32) + late_in[t, 1].astype(f32)
            ).astype(bf)
            pass_rows(first)

    def query_sib(i):
        with scope("dq_sib"):
            for a in range(i * split, (i + 1) * split):
                cols = pl.ds(a * tok, tok)
                dq = jnp.dot(kt[1], ds_sib[:tok, cols], preferred_element_type=f32) + jnp.dot(
                    kt[far], ds_sib[tok:, cols], preferred_element_type=f32
                )
                dq_out[a] = (dq * scale).astype(bf)
        send_dq[i].start()

    for group in groups[:2]:
        join_rows(*group)
    query_sib(0)
    query_sib(1)
    for group in groups[2:]:
        join_rows(*group)
    with scope("dk0"):
        key = (dk_acc[0] + dk_part(ds_own, 0, 0)) * scale
    join_late()

    with scope("dq_own"):
        for i in range(2):
            send_dq[i].wait_recv()
            for a in range(i * split, (i + 1) * split):
                dq = sum(
                    jnp.dot(
                        kt[d],
                        ds_own[d * tok : (d + 1) * tok, a * tok : (a + 1) * tok],
                        preferred_element_type=f32,
                    )
                    for d in range(SPAN)
                )
                dq = dq * scale + dq_in[a].astype(f32)
                qg_ref[:, a * hd : (a + 1) * hd] = dq.T.astype(bf)

    with scope("dk_wait"):
        each_count(ahead, lambda rows: all_of(dki.at[rows], dk_recv).wait())
    for d in range(BACK):
        key = key + dki[d].astype(f32)
    kg_ref[...] = key.astype(bf)

    with scope("rs_wait"):

        ri[pl.ds(mine, 1)] = zo[pl.ds(mine, 1)]
        all_of(ri.at[pl.ds(0, pairs - 1)], rs_recv).wait()
    wg_ref[...] = jnp.sum(ri[...].astype(f32), 0)

    with scope("send_wait"):
        each_count(ahead, lambda rows: all_of(kvw.at[:, rows], kv_send).wait())
        each_count(behind, lambda rows: all_of(back_out.at[:, rows], back_send).wait())
        all_of(q6, sib_send.at[0]).wait()
        send_lse.wait_send()
        send_bias.wait_send()
        send_x.wait_send()
        all_of(lse_s, sib_send.at[4]).wait()
        all_of(dq_out, sib_send.at[5]).wait()
        for dt in range(1, nt):
            all_of(x_t.at[early], x_send.at[dt - 1]).wait()
        all_of(vall.at[pl.ds(0, 2 * nt - 1)], vg_send).wait()
        all_of(late, late_send).wait()
        all_of(po.at[pl.ds(0, (nt + 1) * hh), 0], y_send).wait()
        all_of(ri.at[pl.ds(0, pairs - 1)], rs_send).wait()


def finish(*refs):
    count = len(refs) // 2
    sems = refs[-1]
    copies = [
        pltpu.make_async_copy(refs[i], refs[count + i], sems.at[i]) for i in range(count)
    ]
    for copy in copies:
        copy.start()
    for copy in copies:
        copy.wait()


def shards(nk, nt, queries, keys, values, log_sums, out_grad, chosen, inputs):
    tok, hd = keys.shape
    heads = queries.shape[1] // hd
    nblk = chosen.shape[0]
    feats = inputs.shape[1]
    rw = feats * nt // nk
    per_tp = feats // (2 * rw)
    bf, f32 = jnp.bfloat16, jnp.float32
    dma = pltpu.SemaphoreType.DMA
    vmem = pl.BlockSpec(memory_space=pltpu.VMEM)
    hbm = pl.BlockSpec(memory_space=pltpu.HBM)
    pairs = nk // 4
    parts = pl.pallas_call(
        functools.partial(kernel, nk, nt),
        out_shape=(
            pltpu.VMEM((tok, heads * hd), bf),
            pltpu.VMEM((tok, hd), bf),
            pltpu.VMEM((tok, hd), bf),
            pltpu.VMEM((rw, hd), f32),
        ),
        in_specs=[hbm] * 7,
        out_specs=(vmem, vmem, vmem, vmem),
        scratch_shapes=[
            pltpu.SMEM(chosen.shape, jnp.int32),
            pltpu.VMEM((2, heads, tok), f32),
            pltpu.VMEM((2, heads, tok, hd), bf),
            pltpu.VMEM((2, heads, tok, hd), bf),
            pltpu.VMEM((tok, feats), bf),
            pltpu.VMEM((2, SPAN, tok, hd), bf),
            pltpu.VMEM((SPAN, hd, tok), bf),
            pltpu.VMEM((SPAN, nblk, tok), f32),
            pltpu.VMEM((2, nblk, tok), f32),
            pltpu.VMEM((2, nblk, tok), f32),
            pltpu.VMEM((tok, tok), f32),
            pltpu.VMEM((heads, SPAN + 2, tok, tok), f32),
            pltpu.VMEM((heads, 2, tok, tok), f32),
            pltpu.VMEM((2, tok, heads * tok), bf),
            pltpu.VMEM((SPAN * tok, heads * tok), bf),
            pltpu.VMEM((2 * tok, heads * tok), bf),
            pltpu.VMEM((tok, hd), f32),
            pltpu.VMEM((tok, hd), f32),
            pltpu.VMEM((BACK, tok, hd), f32),
            pltpu.VMEM((2, BACK, tok, hd), bf),
            pltpu.VMEM((2, BACK, tok, hd), bf),
            pltpu.VMEM((heads, tok), f32),
            pltpu.VMEM((heads, tok), f32),
            pltpu.VMEM((heads, tok), f32),
            pltpu.VMEM((heads, tok), f32),
            pltpu.VMEM((heads, hd, tok), bf),
            pltpu.VMEM((heads, hd, tok), bf),
            pltpu.VMEM((per_tp, 2, rw, tok), bf),
            pltpu.VMEM((nt, 2, per_tp, rw, tok), bf),
            pltpu.VMEM((2 * nt, tok, hd), bf),
            pltpu.VMEM((nt - 1, per_tp // 4, 2, rw, hd), bf),
            pltpu.VMEM((nt, 2, per_tp // 4, rw, hd), bf),
            pltpu.VMEM((pairs, 2, rw, hd), f32),
            pltpu.VMEM((pairs, 2, rw, hd), bf),
            pltpu.VMEM((pairs, rw, hd), bf),
            pltpu.VMEM((pairs, rw, hd), bf),
            pltpu.VMEM((pairs, rw, hd), bf),
            dma((7,)),
            dma,
            dma((BACK,)),
            dma,
            dma,
            dma,
            dma,
            dma((6,)),
            dma((8,)),
            dma((nt - 1,)),
            dma((nt - 1,)),
            dma,
            dma((2 * nt,)),
            dma,
            dma((nt - 1,)),
            dma,
            dma((nt + 1,)),
            dma,
            dma,
            pltpu.SemaphoreType.REGULAR((2,)),
        ],
        compiler_params=pltpu.CompilerParams(
            collective_id=0, has_side_effects=True, vmem_limit_bytes=60 * 1024 * 1024
        ),
    )(chosen, log_sums, keys, values, queries, out_grad, inputs)
    return pl.pallas_call(
        finish,
        out_shape=tuple(jax.ShapeDtypeStruct(part.shape, part.dtype) for part in parts),
        in_specs=[vmem] * len(parts),
        out_specs=(hbm,) * len(parts),
        scratch_shapes=[dma((len(parts),))],
    )(*(pltpu.with_memory_space_constraint(part, pltpu.VMEM) for part in parts))


def solution(mesh):
    in_specs = (
        P("kv", "tp"),
        P("kv", "tp"),
        P("kv", "tp"),
        P("tp", "kv"),
        P("kv", "tp"),
        P("kv", "tp", None),
        P("kv", "tp"),
    )
    out_specs = (P("kv", "tp"), P("kv", "tp"), P("kv", "tp"), P("kv", "tp"))
    return jax.shard_map(
        functools.partial(shards, mesh.shape["kv"], mesh.shape["tp"]),
        mesh=mesh,
        in_specs=in_specs,
        out_specs=out_specs,
        check_vma=False,
    )
```

time: 32.8 us -> 28.2 us (0.86)
  the two profiles are of different devices: /device:TPU:14 before, /device:TPU:0 now
where the time goes in v2:
time: 28.2 us; the launch traced here: 28.1 us
  Pallas kernels  27.4 us (97%)
  between operations  0.64 us (2%)
    pallas_call x1, Pallas kernels, shards(): pl.pallas_call(functools.partial(kernel, nk, nt), out_shape=(pltpu.VMEM((...  26.6 us
    pallas_call x1, Pallas kernels, shards(): pl.pallas_call(finish, out_shape=tuple((jax.ShapeDtypeStruct(part.shape,...  0.85 us

profile of v2, /device:TPU:0, one launch (start us, length us, event | category | flops | bytes accessed | tf_op | source)
XLA Modules:
  0.0 28.1 jit_solution(2147552809001504895)
XLA Ops:
  0.6 26.6 %shard_map.102 = (bf16[256,768]{1,0:T(8,128)(2,1)S(1)}, bf16[256,128]{1,0:T(8,128)(2,1)S(1)}, bf16[256,128]{1,0:T(8,128)(2,1)S(1)}, f32[192,128]{1,0:T(8,128)S(1)}) custom-call(s32[4,1,8]{2,1,0:T(1,128)} %chosen_hbm.1, f32[6,256]{1,0:T(8,128)} %lse_hbm.1, bf16[256,128]{1,0:T(8,128)(2,1)} %k_hbm.1, bf16[256,128]{1,0:T(8,128)(2,1)} %v_hbm.1, ...), custom_call_target="tpu_custom_call" | custom-call | tf_op jit(solution)/shard_map/pallas_call | solution.py:687
  27.2 0.9 %shard_map.103 = (bf16[256,768]{1,0:T(8,128)(2,1)}, bf16[256,128]{1,0:T(8,128)(2,1)}, bf16[256,128]{1,0:T(8,128)(2,1)}, f32[192,128]{1,0:T(8,128)}) custom-call(bf16[256,768]{1,0:T(8,128)(2,1)S(1)} %get-tuple-element.8.refs_0_, bf16[256,128]{1,0:T(8,128)(2,1)S(1)} %get-tuple-element.9.refs_1_, bf16[256,128]{1,0:T(8,128)(2,1)S(1)} %get-tuple-element.10.refs_2_, ...), custom_call_target="tpu_custom_call" | custom-call | tf_op jit(solution)/shard_map/pallas_call | solution.py:760

commit v3 on v2

--- a/solution.py
+++ b/solution.py
@@ -55,6 +55,8 @@
     dk_acc,
     back_out,
     back_in,
+    dk_pass,
+    dk_far2,
     dl_out,
     dl_in,
     dt_out,
@@ -78,6 +80,7 @@
     back_send,
     dv_recv,
     dk_recv,
+    pass_recv,
     sib_send,
     sib_recv,
     x_send,
@@ -314,7 +317,14 @@
         @pl.when(chip + d >= chips)
         def _():
             dvi[d - 1] = zero
-            dki[d - 1] = zero
+
+    @pl.when(side == 1)
+    def _():
+        dki[0] = zero
+
+    @pl.when(ahead < 2)
+    def _():
+        dki[1] = zero
 
     def weights(whose, slot, d, bias, buf):
         keys = kw[d]
@@ -431,10 +441,9 @@
     my_vg = vall.at[tp * 2 + core]
     vg_copies = [remote(my_vg, my_vg, vg_send, vg_recv.at[tp * 2 + core], sib)]
     for dt in range(1, nt):
-        for kv in (me, sib):
-            vg_copies.append(
-                remote(my_vg, my_vg, vg_send, vg_recv.at[tp * 2 + core], kv, lax.rem(tp + dt, nt))
-            )
+        vg_copies.append(
+            remote(my_vg, my_vg, vg_send, vg_recv.at[tp * 2 + core], me, lax.rem(tp + dt, nt))
+        )
     for copy in vg_copies:
         copy.start()
 
@@ -545,6 +554,12 @@
             put_rows(dt, first, part)
             groups.append((dt, first))
 
+    for dt in range(1, nt):
+        i = lax.rem(tp + dt, nt) * 2 + core
+        with scope("vg_x_wait"):
+            all_of(vall.at[i], vg_recv.at[i]).wait()
+        remote(vall.at[i], vall.at[i], vg_send, vg_recv.at[i], sib).start()
+
     with scope("dt_wait"):
         send_dt.wait_recv()
     with scope("sib_ds"):
@@ -557,13 +572,28 @@
     with scope("dk_sib"):
         dko[0] = ((dk_acc[0] + dk_part(ds_sib, 0, 1)) * scale).astype(bf)
         dk_far = dk_part(ds_sib, 1, 1)
-        dko[1] = ((dk_acc[1] + jnp.where(core == 1, dk_far, 0.0)) * scale).astype(bf)
+        dk_far2[...] = (dk_acc[1] + jnp.where(core == 1, dk_far, 0.0)) * scale
         dk_acc[0] = jnp.where(core == 0, dk_far, 0.0)
-    for d in range(1, SPAN):
-
-        @pl.when(chip >= d)
-        def _():
-            dk_copy(d).start()
+    merge = (side == 1) & (chip >= 3)
+    hand = remote(dko.at[0], dk_pass, back_send, pass_recv, across)
+
+    @pl.when(side == 1)
+    def _():
+        dk_copy(1).start()
+
+    @pl.when((side == 0) & (chip >= 2))
+    def _():
+        hand.start()
+        dko[1] = dk_far2[...].astype(bf)
+        dk_copy(2).start()
+
+    def merge_key():
+        @pl.when(merge)
+        def _():
+            with scope("pass_wait"):
+                hand.wait_recv()
+            dko[1] = (dk_far2[...] + dk_pass[...].astype(f32)).astype(bf)
+            dk_copy(2).start()
 
     def late_copy(dt, i):
         return remote(
@@ -578,8 +608,7 @@
     for dt in range(1, nt):
         t = lax.rem(tp + dt, nt)
         with scope("vg_other_wait"):
-            vg_wait(t, 0)
-            vg_wait(t, 1)
+            vg_wait(t, 1 - core)
         with scope("w_late"):
             late[dt - 1] = own_rows(mid * half, t).astype(bf).reshape(hh, 2, rw, hd)
             for i in (1, 0):
@@ -614,6 +643,7 @@
         join_rows(*group)
     with scope("dk0"):
         key = (dk_acc[0] + dk_part(ds_own, 0, 0)) * scale
+    merge_key()
     join_late()
 
     with scope("dq_own"):
@@ -632,7 +662,15 @@
                 qg_ref[:, a * hd : (a + 1) * hd] = dq.T.astype(bf)
 
     with scope("dk_wait"):
-        each_count(ahead, lambda rows: all_of(dki.at[rows], dk_recv).wait())
+
+        @pl.when((side == 0) & (ahead >= 2))
+        def _():
+            all_of(dki, dk_recv).wait()
+
+        @pl.when((side == 0) != (ahead >= 2))
+        def _():
+            all_of(dki.at[0], dk_recv).wait()
+
     for d in range(BACK):
         key = key + dki[d].astype(f32)
     kg_ref[...] = key.astype(bf)
@@ -716,6 +754,8 @@
             pltpu.VMEM((BACK, tok, hd), f32),
             pltpu.VMEM((2, BACK, tok, hd), bf),
             pltpu.VMEM((2, BACK, tok, hd), bf),
+            pltpu.VMEM((tok, hd), bf),
+            pltpu.VMEM((tok, hd), f32),
             pltpu.VMEM((heads, tok), f32),
             pltpu.VMEM((heads, tok), f32),
             pltpu.VMEM((heads, tok), f32),
@@ -735,6 +775,7 @@
             dma((7,)),
             dma,
             dma((BACK,)),
+            dma,
             dma,
             dma,
             dma,

time: 28.2 us -> 27.1 us (0.961)
  the two profiles are of different devices: /device:TPU:0 before, /device:TPU:14 now
where the time goes in v3:
time: 27.1 us; the launch traced here: 26.6 us
  Pallas kernels  25.9 us (96%)
  between operations  0.64 us (2%)
    pallas_call x1, Pallas kernels, shards(): pl.pallas_call(functools.partial(kernel, nk, nt), out_shape=(pltpu.VMEM((...  25.1 us
    pallas_call x1, Pallas kernels, shards(): pl.pallas_call(finish, out_shape=tuple((jax.ShapeDtypeStruct(part.shape,...  0.85 us

profile of v3, /device:TPU:14, one launch (start us, length us, event | category | flops | bytes accessed | tf_op | source)
XLA Modules:
  0.0 26.6 jit_solution(16236102409743441529)
XLA Ops:
  0.6 25.1 %shard_map.102 = (bf16[256,768]{1,0:T(8,128)(2,1)S(1)}, bf16[256,128]{1,0:T(8,128)(2,1)S(1)}, bf16[256,128]{1,0:T(8,128)(2,1)S(1)}, f32[192,128]{1,0:T(8,128)S(1)}) custom-call(s32[4,1,8]{2,1,0:T(1,128)} %chosen_hbm.1, f32[6,256]{1,0:T(8,128)} %lse_hbm.1, bf16[256,128]{1,0:T(8,128)(2,1)} %k_hbm.1, bf16[256,128]{1,0:T(8,128)(2,1)} %v_hbm.1, ...), custom_call_target="tpu_custom_call" | custom-call | tf_op jit(solution)/shard_map/pallas_call | solution.py:725
  25.7 0.9 %shard_map.103 = (bf16[256,768]{1,0:T(8,128)(2,1)}, bf16[256,128]{1,0:T(8,128)(2,1)}, bf16[256,128]{1,0:T(8,128)(2,1)}, f32[192,128]{1,0:T(8,128)}) custom-call(bf16[256,768]{1,0:T(8,128)(2,1)S(1)} %get-tuple-element.8.refs_0_, bf16[256,128]{1,0:T(8,128)(2,1)S(1)} %get-tuple-element.9.refs_1_, bf16[256,128]{1,0:T(8,128)(2,1)S(1)} %get-tuple-element.10.refs_2_, ...), custom_call_target="tpu_custom_call" | custom-call | tf_op jit(solution)/shard_map/pallas_call | solution.py:801

commit v4 on v3

--- a/solution.py
+++ b/solution.py
@@ -635,12 +635,12 @@
                 dq_out[a] = (dq * scale).astype(bf)
         send_dq[i].start()
 
-    for group in groups[:2]:
-        join_rows(*group)
+    join_rows(*groups[0])
     query_sib(0)
-    query_sib(1)
     for group in groups[2:]:
         join_rows(*group)
+    join_rows(*groups[1])
+    query_sib(1)
     with scope("dk0"):
         key = (dk_acc[0] + dk_part(ds_own, 0, 0)) * scale
     merge_key()

time: 27.1 us -> 26.9 us (level)
  no operation moved by 1% of the time
where the time goes in v4:
time: 26.9 us; the launch traced here: 26.4 us
  Pallas kernels  25.7 us (96%)
  between operations  0.64 us (2%)
    pallas_call x1, Pallas kernels, shards(): pl.pallas_call(functools.partial(kernel, nk, nt), out_shape=(pltpu.VMEM((...  24.9 us
    pallas_call x1, Pallas kernels, shards(): pl.pallas_call(finish, out_shape=tuple((jax.ShapeDtypeStruct(part.shape,...  0.85 us

profile of v4, /device:TPU:14, one launch (start us, length us, event | category | flops | bytes accessed | tf_op | source)
XLA Modules:
  0.0 26.4 jit_solution(8512355263913019102)
XLA Ops:
  0.6 24.9 %shard_map.102 = (bf16[256,768]{1,0:T(8,128)(2,1)S(1)}, bf16[256,128]{1,0:T(8,128)(2,1)S(1)}, bf16[256,128]{1,0:T(8,128)(2,1)S(1)}, f32[192,128]{1,0:T(8,128)S(1)}) custom-call(s32[4,1,8]{2,1,0:T(1,128)} %chosen_hbm.1, f32[6,256]{1,0:T(8,128)} %lse_hbm.1, bf16[256,128]{1,0:T(8,128)(2,1)} %k_hbm.1, bf16[256,128]{1,0:T(8,128)(2,1)} %v_hbm.1, ...), custom_call_target="tpu_custom_call" | custom-call | tf_op jit(solution)/shard_map/pallas_call | solution.py:725
  25.5 0.9 %shard_map.103 = (bf16[256,768]{1,0:T(8,128)(2,1)}, bf16[256,128]{1,0:T(8,128)(2,1)}, bf16[256,128]{1,0:T(8,128)(2,1)}, f32[192,128]{1,0:T(8,128)}) custom-call(bf16[256,768]{1,0:T(8,128)(2,1)S(1)} %get-tuple-element.8.refs_0_, bf16[256,128]{1,0:T(8,128)(2,1)S(1)} %get-tuple-element.9.refs_1_, bf16[256,128]{1,0:T(8,128)(2,1)S(1)} %get-tuple-element.10.refs_2_, ...), custom_call_target="tpu_custom_call" | custom-call | tf_op jit(solution)/shard_map/pallas_call | solution.py:801

commit v5 on v4

--- a/solution.py
+++ b/solution.py
@@ -123,7 +123,7 @@
     ahead = chips - 1 - chip
     near_chips = [(step, ahead >= step if step > 0 else behind >= -step) for step in STEPS]
     barrier = pltpu.get_barrier_semaphore()
-    count = 1 + 3 * (nt - 1)
+    count = 1 + 2 * (nt - 1)
     for step, exists in near_chips:
         count = count + jnp.where(exists, 1, 0)
 
@@ -135,7 +135,7 @@
 
     pl.semaphore_signal(barrier, inc=1, device_id=(sib, tp), device_id_type=MESH)
     for dt in range(1, nt):
-        for kv in (me, sib, across):
+        for kv in (me, sib):
             pl.semaphore_signal(
                 barrier, inc=1, device_id=(kv, lax.rem(tp + dt, nt)), device_id_type=MESH
             )
@@ -213,6 +213,10 @@
 
     with scope("barrier_wait"):
         pl.semaphore_wait(barrier, count)
+    for dt in range(1, nt):
+        pl.semaphore_signal(
+            go_sem.at[2], inc=1, device_id=(me, lax.rem(tp + dt, nt)), device_id_type=MESH
+        )
 
     def relay(point):
         for i, step, left, done in ((0, -BACK, ahead, behind), (1, BACK, behind, ahead)):
@@ -292,7 +296,9 @@
     x_copies = []
     for dt in range(1, nt):
         other = lax.rem(tp + dt, nt)
-        for s, kv, par in ((0, me, core), (1, sib, 1 - core)):
+        for s in range(2):
+            par = 1 - s
+            kv = me + par - core
             x_copies.append(
                 remote(
                     x_t.at[early, par],
@@ -605,6 +611,7 @@
             lax.rem(tp + dt, nt),
         )
 
+    pl.semaphore_wait(go_sem.at[2], nt - 1)
     for dt in range(1, nt):
         t = lax.rem(tp + dt, nt)
         with scope("vg_other_wait"):
@@ -792,7 +799,7 @@
             dma((nt + 1,)),
             dma,
             dma,
-            pltpu.SemaphoreType.REGULAR((2,)),
+            pltpu.SemaphoreType.REGULAR((3,)),
         ],
         compiler_params=pltpu.CompilerParams(
             collective_id=0, has_side_effects=True, vmem_limit_bytes=60 * 1024 * 1024

time: 26.9 us -> 26.6 us (0.989); the launches traced: 26.4 us -> 26.5 us
  no operation moved by 1% of the time
where the time goes in v5:
time: 26.6 us; the launch traced here: 26.5 us
  Pallas kernels  25.8 us (97%)
  between operations  0.64 us (2%)
    pallas_call x1, Pallas kernels, shards(): pl.pallas_call(functools.partial(kernel, nk, nt), out_shape=(pltpu.VMEM((...  25 us
    pallas_call x1, Pallas kernels, shards(): pl.pallas_call(finish, out_shape=tuple((jax.ShapeDtypeStruct(part.shape,...  0.85 us

profile of v5, /device:TPU:14, one launch (start us, length us, event | category | flops | bytes accessed | tf_op | source)
XLA Modules:
  0.0 26.5 jit_solution(5602446647741018617)
XLA Ops:
  0.6 25.0 %shard_map.102 = (bf16[256,768]{1,0:T(8,128)(2,1)S(1)}, bf16[256,128]{1,0:T(8,128)(2,1)S(1)}, bf16[256,128]{1,0:T(8,128)(2,1)S(1)}, f32[192,128]{1,0:T(8,128)S(1)}) custom-call(s32[4,1,8]{2,1,0:T(1,128)} %chosen_hbm.1, f32[6,256]{1,0:T(8,128)} %lse_hbm.1, bf16[256,128]{1,0:T(8,128)(2,1)} %k_hbm.1, bf16[256,128]{1,0:T(8,128)(2,1)} %v_hbm.1, ...), custom_call_target="tpu_custom_call" | custom-call | tf_op jit(solution)/shard_map/pallas_call | solution.py:732
  25.6 0.9 %shard_map.103 = (bf16[256,768]{1,0:T(8,128)(2,1)}, bf16[256,128]{1,0:T(8,128)(2,1)}, bf16[256,128]{1,0:T(8,128)(2,1)}, f32[192,128]{1,0:T(8,128)}) custom-call(bf16[256,768]{1,0:T(8,128)(2,1)S(1)} %get-tuple-element.8.refs_0_, bf16[256,128]{1,0:T(8,128)(2,1)S(1)} %get-tuple-element.9.refs_1_, bf16[256,128]{1,0:T(8,128)(2,1)S(1)} %get-tuple-element.10.refs_2_, ...), custom_call_target="tpu_custom_call" | custom-call | tf_op jit(solution)/shard_map/pallas_call | solution.py:808

commit v6 on v5

--- a/solution.py
+++ b/solution.py
@@ -74,10 +74,8 @@
     zo,
     ri,
     ld_sem,
-    kv_send,
     k_recv,
     v_recv,
-    back_send,
     dv_recv,
     dk_recv,
     pass_recv,
@@ -122,6 +120,8 @@
     behind = chip
     ahead = chips - 1 - chip
     near_chips = [(step, ahead >= step if step > 0 else behind >= -step) for step in STEPS]
+    kv_send, back_send = ld_sem.at[0], ld_sem.at[1]
+    sib_sends = [ld_sem.at[i] for i in (5, 4, 3, 6)] + [sib_send.at[0], sib_send.at[1]]
     barrier = pltpu.get_barrier_semaphore()
     count = 1 + 2 * (nt - 1)
     for step, exists in near_chips:
@@ -197,7 +197,7 @@
                 wait(pl.ds(0, count))
 
     def to_sib(i, j, src, dst):
-        return remote(src, dst, sib_send.at[i], sib_recv.at[j], sib)
+        return remote(src, dst, sib_sends[i], sib_recv.at[j], sib)
 
     send_q = to_sib(0, 0, q6.at[0], q6.at[1])
     send_do = to_sib(0, 0, do6.at[0], do6.at[1])
@@ -601,12 +601,19 @@
             dko[1] = (dk_far2[...] + dk_pass[...].astype(f32)).astype(bf)
             dk_copy(2).start()
 
-    def late_copy(dt, i):
+    if hh % 2 == 0:
+        chunks = [(c * hh // 2, hh // 2, pl.ds(0, rw)) for c in range(2)]
+    else:
+        chunks = [(0, hh, pl.ds(c * rw // 2, rw // 2)) for c in range(2)]
+
+    def late_copy(dt, c, i):
+        start, count, rows = chunks[c]
+        blocks = pl.ds(start, count)
         return remote(
-            late.at[dt - 1, :, side if i == 0 else 1 - side],
-            late_in.at[tp, side],
+            late.at[dt - 1, blocks, side if i == 0 else 1 - side, rows],
+            late_in.at[tp, side, blocks, rows],
             late_send,
-            late_recv.at[nt - dt - 1],
+            late_recv.at[nt - dt - 1, c],
             me if i == 0 else across,
             lax.rem(tp + dt, nt),
         )
@@ -618,19 +625,35 @@
             vg_wait(t, 1 - core)
         with scope("w_late"):
             late[dt - 1] = own_rows(mid * half, t).astype(bf).reshape(hh, 2, rw, hd)
-            for i in (1, 0):
-                late_copy(dt, i).start()
-
-    def join_late():
+            for c in range(2):
+                for i in (1, 0):
+                    late_copy(dt, c, i).start()
+
+    def join_late(c):
+        start, count, rows = chunks[c]
+        blocks = pl.ds(start, count)
         for dt in range(1, nt):
             t = lax.rem(tp + dt, nt)
-            first = t * per_tp + (1 - lax.rem(t, 2)) * half
+            first = (t * per_tp + (1 - lax.rem(t, 2)) * half) // 2 + start
             with scope("late_wait"):
-                all_of(late_in.at[t], late_recv.at[dt - 1]).wait()
-            zo[pl.ds(first // 2, hh)] = (
-                late_in[t, 0].astype(f32) + late_in[t, 1].astype(f32)
+                all_of(late_in.at[t, :, blocks, rows], late_recv.at[dt - 1, c]).wait()
+            zo[pl.ds(first, count), rows] = (
+                late_in[t, 0, blocks, rows].astype(f32) + late_in[t, 1, blocks, rows].astype(f32)
             ).astype(bf)
-            pass_rows(first)
+
+            @pl.loop(0, count)
+            def _(j):
+                m = first + j
+
+                @pl.when(m != mine)
+                def _():
+                    remote(
+                        zo.at[m, rows],
+                        ri.at[mine, rows],
+                        rs_send,
+                        rs_recv,
+                        (2 * m + side) * 2 + core,
+                    ).start()
 
     def query_sib(i):
         with scope("dq_sib"):
@@ -651,7 +674,8 @@
     with scope("dk0"):
         key = (dk_acc[0] + dk_part(ds_own, 0, 0)) * scale
     merge_key()
-    join_late()
+    for c in range(2):
+        join_late(c)
 
     with scope("dq_own"):
         for i in range(2):
@@ -691,12 +715,12 @@
     with scope("send_wait"):
         each_count(ahead, lambda rows: all_of(kvw.at[:, rows], kv_send).wait())
         each_count(behind, lambda rows: all_of(back_out.at[:, rows], back_send).wait())
-        all_of(q6, sib_send.at[0]).wait()
+        all_of(q6, sib_sends[0]).wait()
         send_lse.wait_send()
         send_bias.wait_send()
         send_x.wait_send()
-        all_of(lse_s, sib_send.at[4]).wait()
-        all_of(dq_out, sib_send.at[5]).wait()
+        all_of(lse_s, sib_sends[4]).wait()
+        all_of(dq_out, sib_sends[5]).wait()
         for dt in range(1, nt):
             all_of(x_t.at[early], x_send.at[dt - 1]).wait()
         all_of(vall.at[pl.ds(0, 2 * nt - 1)], vg_send).wait()
@@ -780,21 +804,19 @@
             pltpu.VMEM((pairs, rw, hd), bf),
             pltpu.VMEM((pairs, rw, hd), bf),
             dma((7,)),
-            dma,
             dma((BACK,)),
             dma,
             dma,
             dma,
             dma,
-            dma,
-            dma((6,)),
+            dma((2,)),
             dma((8,)),
             dma((nt - 1,)),
             dma((nt - 1,)),
             dma,
             dma((2 * nt,)),
             dma,
-            dma((nt - 1,)),
+            dma((nt - 1, 2)),
             dma,
             dma((nt + 1,)),
             dma,

time: 26.6 us -> 26.5 us (level)
  no operation moved by 1% of the time
where the time goes in v6:
time: 26.5 us; the launch traced here: 26.4 us
  Pallas kernels  25.7 us (97%)
  between operations  0.64 us (2%)
    pallas_call x1, Pallas kernels, shards(): pl.pallas_call(functools.partial(kernel, nk, nt), out_shape=(pltpu.VMEM((...  24.9 us
    pallas_call x1, Pallas kernels, shards(): pl.pallas_call(finish, out_shape=tuple((jax.ShapeDtypeStruct(part.shape,...  0.85 us

profile of v6, /device:TPU:14, one launch (start us, length us, event | category | flops | bytes accessed | tf_op | source)
XLA Modules:
  0.0 26.4 jit_solution(961632981571943577)
XLA Ops:
  0.6 24.9 %shard_map.102 = (bf16[256,768]{1,0:T(8,128)(2,1)S(1)}, bf16[256,128]{1,0:T(8,128)(2,1)S(1)}, bf16[256,128]{1,0:T(8,128)(2,1)S(1)}, f32[192,128]{1,0:T(8,128)S(1)}) custom-call(s32[4,1,8]{2,1,0:T(1,128)} %chosen_hbm.1, f32[6,256]{1,0:T(8,128)} %lse_hbm.1, bf16[256,128]{1,0:T(8,128)(2,1)} %k_hbm.1, bf16[256,128]{1,0:T(8,128)(2,1)} %v_hbm.1, ...), custom_call_target="tpu_custom_call" | custom-call | tf_op jit(solution)/shard_map/pallas_call | solution.py:756
  25.5 0.9 %shard_map.103 = (bf16[256,768]{1,0:T(8,128)(2,1)}, bf16[256,128]{1,0:T(8,128)(2,1)}, bf16[256,128]{1,0:T(8,128)(2,1)}, f32[192,128]{1,0:T(8,128)}) custom-call(bf16[256,768]{1,0:T(8,128)(2,1)S(1)} %get-tuple-element.8.refs_0_, bf16[256,128]{1,0:T(8,128)(2,1)S(1)} %get-tuple-element.9.refs_1_, bf16[256,128]{1,0:T(8,128)(2,1)S(1)} %get-tuple-element.10.refs_2_, ...), custom_call_target="tpu_custom_call" | custom-call | tf_op jit(solution)/shard_map/pallas_call | solution.py:830
